TPU v7x, 32 devices: a whole 2x2x4 slice. The times are simulated.
32 devices in a mesh: sp: 8 (over z, x), tp: 4 (over y, core).
Axes of the slice: x: 2, y: 2, z: 4, core: 2. Of those that a mesh axis runs over, the one named last changes fastest.
Arguments:
- residual_in: bfloat16 [1536, 2048], P('sp', 'tp'), may hold values from -6 to 6
- query_rows: bfloat16 [1536, 1024], P('sp', 'tp'), may hold values from -8 to 8
- key_rows: bfloat16 [1536, 1024], P('sp', 'tp'), may hold values from -8 to 8
- value_rows: bfloat16 [1536, 1024], P('sp', 'tp'), may hold values from -6 to 6
- map_weight: float32 [16], P('tp'), may hold values from 0.3 to 0.8
- head_gain: float32 [64], replicated, may hold values from 0.1 to 1.9
- out_proj: bfloat16 [1024, 2048], P(None, 'tp'), may hold values from -0.1875 to 0.1875
- norm_gain: float32 [2048], replicated, may hold values from 0.1 to 1.9
- route_ids: int32 [1536, 2], P('sp'), may hold values from 0 to 7, all different within a row; in each aligned block of 192 rows (0 to 191, 192 to 383, ...) at most 60 rows name the same one
- route_weights: float32 [1536, 2], P('sp'), may hold values from 0.2 to 1.2
- expert_gate: bfloat16 [8, 1024, 2048], P('sp', 'tp'), may hold values from -0.125 to 0.125
- expert_up: bfloat16 [8, 1024, 2048], P('sp', 'tp'), may hold values from -0.125 to 0.125
- expert_down: bfloat16 [8, 1024, 2048], P('sp', None, 'tp'), may hold values from -0.1875 to 0.1875
- shared_gate: bfloat16 [1024, 2048], P('tp'), may hold values from -0.125 to 0.125
- shared_up: bfloat16 [1024, 2048], P('tp'), may hold values from -0.125 to 0.125
- shared_down: bfloat16 [1024, 2048], P(None, 'tp'), may hold values from -0.1875 to 0.1875
Outputs:
- mixed_out: bfloat16 [1536, 2048], P('sp', 'tp')
Inputs may be any that keep to these rules, and one draw needn't show every extreme that they name: `route_ids`: each row names 2 different experts. Among the rows held by one index of sp no expert is named more than 60 times, and in every draw some expert is named exactly 60 times by the rows of some index of sp.
All inputs are finite; a program needn't handle non-finite values.
Results may differ from a plain program's by a relative error of at most 0.0095.
Values may be sent and summed in bfloat16 or wider, within the bound.
No kernel may reach another device: no remote copies, remote signals or barrier semaphores. Data moves between devices by JAX's collectives and lax.ppermute only.
A program may use at most 64 MiB of HBM per device.

v0:
```python
import jax
import jax.numpy as jnp
from jax import lax
from jax.sharding import PartitionSpec as P

epsilon = 1e-06
masked_score = -1e30


def rms_scale(values, gain_vec):
    squares = jnp.mean(values * values, axis=-1, keepdims=True)
    return values * lax.rsqrt(squares + epsilon) * gain_vec


def block_slots(route_block, experts_all, capacity):
    flat_ids = route_block.reshape(-1)
    one_hot = (flat_ids[:, None] == jnp.arange(experts_all, dtype=jnp.int32)[None, :]).astype(
        jnp.int32
    )
    earlier = jnp.cumsum(one_hot, axis=0) - one_hot
    position = jnp.sum(earlier * one_hot, axis=1)
    return (flat_ids * capacity + position).reshape(route_block.shape)


def body(
    residual_in,
    query_rows,
    key_rows,
    value_rows,
    map_weight,
    head_gain,
    out_proj,
    norm_gain,
    route_ids,
    route_weights,
    expert_gate,
    expert_up,
    expert_down,
    shared_gate,
    shared_up,
    shared_down,
):
    seq_dev = residual_in.shape[0]
    col_dev = residual_in.shape[1]
    heads_here = map_weight.shape[0]
    head_dim = head_gain.shape[0]
    half_dim = head_dim // 2
    topk_count = route_ids.shape[1]
    exp_here = expert_gate.shape[0]
    experts_all = exp_here * lax.axis_size("sp")
    capacity = 5 * seq_dev * topk_count // (4 * experts_all)
    score_scale = half_dim ** (-0.5)
    query_pos = lax.axis_index("sp") * seq_dev + jnp.arange(seq_dev, dtype=jnp.int32)
    query_heads = query_rows.reshape(seq_dev, heads_here, 2, half_dim)
    key_piece = lax.all_gather(key_rows, "sp", axis=0, tiled=True)
    value_piece = lax.all_gather(value_rows, "sp", axis=0, tiled=True)
    piece_len = key_piece.shape[0]
    key_heads = key_piece.reshape(piece_len, heads_here, 2, half_dim)
    value_heads = value_piece.reshape(piece_len, heads_here, head_dim)
    scores = (
        jnp.einsum("qhmd,khmd->mhqk", query_heads, key_heads, preferred_element_type=jnp.float32)
        * score_scale
    )
    key_pos = jnp.arange(piece_len, dtype=jnp.int32)
    visible = key_pos[None, :] <= query_pos[:, None]
    scores = jnp.where(visible, scores, masked_score)
    run_max = jnp.full((2, heads_here, seq_dev), masked_score, jnp.float32)
    new_max = jnp.maximum(run_max, jnp.max(scores, axis=-1))
    expo = jnp.where(visible, jnp.exp(scores - new_max[..., None]), 0.0)
    new_sum = jnp.sum(expo, axis=-1)
    product = jnp.einsum(
        "mhqk,khd->mhqd", expo.astype(jnp.bfloat16), value_heads, preferred_element_type=jnp.float32
    )
    summed = product / new_sum[..., None]
    diff_out = summed[0] - map_weight[:, None, None] * summed[1]
    head_out = rms_scale(diff_out, head_gain).astype(jnp.bfloat16)
    head_out = jnp.transpose(head_out, (1, 0, 2)).reshape(seq_dev, heads_here * head_dim)
    attn = jnp.dot(
        lax.all_gather(head_out, "tp", axis=1, tiled=True),
        out_proj,
        preferred_element_type=jnp.float32,
    )
    hidden_state = (residual_in.astype(jnp.float32) + attn).astype(jnp.bfloat16)
    full_rows = lax.all_gather(hidden_state, "tp", axis=1, tiled=True)
    normed = rms_scale(full_rows.astype(jnp.float32), norm_gain).astype(jnp.bfloat16)
    shared_gate_part = jnp.einsum(
        "rd,fd->rf", normed, shared_gate, preferred_element_type=jnp.float32
    )
    shared_up_part = jnp.einsum("rd,fd->rf", normed, shared_up, preferred_element_type=jnp.float32)
    shared_hidden = (jax.nn.silu(shared_gate_part) * shared_up_part).astype(jnp.bfloat16)
    slot_ids = block_slots(route_ids, experts_all, capacity)
    token_of = jnp.repeat(jnp.arange(seq_dev, dtype=jnp.int32), topk_count)
    slot_token = (
        jnp.full((experts_all * capacity,), seq_dev, jnp.int32)
        .at[slot_ids.reshape(-1)]
        .set(token_of)
    )
    own_cols = lax.dynamic_slice_in_dim(normed, lax.axis_index("tp") * col_dev, col_dev, 1)
    padded = jnp.concatenate([own_cols, jnp.zeros((1, col_dev), jnp.bfloat16)], axis=0)
    outgoing = jnp.take(padded, slot_token, axis=0).reshape(experts_all, capacity, col_dev)
    arrived = lax.all_to_all(outgoing, "sp", split_axis=0, concat_axis=1, tiled=True)
    arrived_rows = arrived.shape[1]
    pieces = lax.all_gather(arrived, "tp", axis=2, tiled=True)
    gate_add = jnp.einsum("erd,efd->erf", pieces, expert_gate, preferred_element_type=jnp.float32)
    up_add = jnp.einsum("erd,efd->erf", pieces, expert_up, preferred_element_type=jnp.float32)
    expert_hidden = (jax.nn.silu(gate_add) * up_add).astype(jnp.bfloat16)
    expert_flat = expert_hidden.reshape(exp_here * arrived_rows, expert_hidden.shape[2])
    pieces = (
        lax.all_gather(shared_hidden, "tp", axis=1, tiled=True),
        lax.all_gather(expert_flat, "tp", axis=1, tiled=True),
    )
    piece_width = pieces[0].shape[1]
    routed_piece = pieces[1].reshape(exp_here, arrived_rows, piece_width)
    shared_add = jnp.dot(pieces[0], shared_down, preferred_element_type=jnp.float32)
    expert_add = jnp.einsum(
        "erf,efd->erd", routed_piece, expert_down, preferred_element_type=jnp.float32
    )
    returned_rows = lax.all_to_all(
        expert_add.astype(jnp.bfloat16), "sp", split_axis=1, concat_axis=0, tiled=True
    )
    returned_flat = returned_rows.reshape(experts_all * capacity, col_dev)
    picked = (
        jnp.take(returned_flat, slot_ids.reshape(-1), axis=0)
        .reshape(seq_dev, topk_count, col_dev)
        .astype(jnp.float32)
    )
    routed = jnp.sum(picked * route_weights[:, :, None], axis=1)
    return (hidden_state.astype(jnp.float32) + shared_add + routed).astype(jnp.bfloat16)


def solution(mesh):
    in_specs = (
        P("sp", "tp"),
        P("sp", "tp"),
        P("sp", "tp"),
        P("sp", "tp"),
        P("tp"),
        P(),
        P(None, "tp"),
        P(),
        P("sp", None),
        P("sp", None),
        P("sp", "tp", None),
        P("sp", "tp", None),
        P("sp", None, "tp"),
        P("tp", None),
        P("tp", None),
        P(None, "tp"),
    )
    out_specs = P("sp", "tp")
    return jax.shard_map(body, mesh=mesh, in_specs=in_specs, out_specs=out_specs, check_vma=False)
```

profile of v0, /device:TPU:0, one launch (start us, length us, event | category | flops | bytes accessed | tf_op | source)
XLA Modules:
  0.0 206.6 jit_solution(2744693201549045714)
XLA Ops:
  10.1 2.9 %scatter_custom_fusion = s32[480]{0:T(512)S(1)} fusion(s32[384]{0:T(512)S(1)} %fusion.40, s32[384]{0:T(512)S(1)} %reshape.188, s32[]{:T(128)} %constant.26.clone.1), kind=kCustom, calls=%fused_computation.66 | custom fusion | bytes 1924 | tf_op jit(solution)/shard_map/scatter | solution.py:96
  13.3 34.1 %all_gather.21 = bf16[1536,256]{1,0:T(8,128)(2,1)S(1)} all-gather(bf16[192,256]{1,0:T(8,128)(2,1)} %param.18), channel_id=1, replica_groups=mesh['sp'=8,'tp'=4] {'sp'}, dimensions={0}, use_global_device_ids=true | all-gather | bytes 884736 | tf_op jit(solution)/shard_map/all_gather | solution.py:55
  47.6 1.0 copy.60
  48.6 1.9 fusion
  50.5 4.4 %fusion.1 = (f32[2,4,192]{2,1,0:T(4,128)S(1)}, bf16[2,4,192,1536]{3,2,1,0:T(8,128)(2,1)}) fusion(f32[2,4,192,1536]{3,2,1,0:T(8,128)S(1)} %get-tuple-element.8, f32[2,4,192]{2,1,0:T(4,128)S(1)} %broadcast_maximum_fusion, pred[192,1536]{1,0:T(8,128)(4,1)S(1)} %iota_compare_fusion), kind=kLoop, calls=%fused_computation.6 | loop fusion | flops 14154240 | bytes 14462976 | tf_op jit(solution)/shard_map/reduce_sum | solution.py:70
  55.0 32.1 %all_gather.22 = bf16[1536,256]{1,0:T(8,128)(2,1)S(1)} all-gather(bf16[192,256]{1,0:T(8,128)(2,1)S(1)} %copy-done.2), channel_id=1, replica_groups=mesh['sp'=8,'tp'=4] {'sp'}, dimensions={0}, use_global_device_ids=true | all-gather | bytes 884736 | tf_op jit(solution)/shard_map/all_gather | solution.py:56
  87.4 4.0 %fusion.29 = f32[2,4,192,64]{2,3,0,1:T(8,128)S(1)} fusion(bf16[1536,4,64,1]{0,2,3,1:T(8,128)(2,1)S(1)} %bitcast.84, bf16[2,4,192,1536]{3,2,1,0:T(8,128)(2,1)} %get-tuple-element.6, f32[2,4,192]{2,0,1:T(2,128)S(1)} %copy.66), kind=kOutput, calls=%fused_computation.35 | convolution fusion | flops 302088192 | bytes 5904384 | tf_op jit(solution)/shard_map/mhqk,khd->mhqd/dot_general | solution.py:71
  91.7 7.2 %all_gather.23 = bf16[192,1024]{0,1:T(8,128)(2,1)S(1)} all-gather(bf16[192,256]{0,1:T(8,128)(2,1)S(1)} %bitcast.85), channel_id=1, replica_groups=mesh['sp'=8,'tp'=4] {'tp'}, dimensions={1}, use_global_device_ids=true | all-gather | bytes 491520 | tf_op jit(solution)/shard_map/all_gather | solution.py:79
  98.9 1.1 fusion.23
  100.0 8.9 %all_gather.24 = bf16[192,2048]{1,0:T(8,128)(2,1)S(1)} all-gather(bf16[192,512]{1,0:T(8,128)(2,1)} %fusion.23), channel_id=1, replica_groups=mesh['sp'=8,'tp'=4] {'tp'}, dimensions={1}, use_global_device_ids=true | all-gather | bytes 983040 | tf_op jit(solution)/shard_map/all_gather | solution.py:84
  109.5 2.1 %gather_fusion = bf16[480,512]{1,0:T(8,128)(2,1)S(1)} fusion(bf16[193,512]{1,0:T(8,128)(2,1)S(1)} %concatenate.3, s32[1024]{0:T(1024)S(1)} %pad_clamp_fusion.1), kind=kCustom, calls=%fused_computation | custom fusion | bytes 984960 | tf_op jit(solution)/shard_map/jit(_take)/gather | solution.py:100
  112.0 20.3 %all_to_all.21 = bf16[8,60,512]{2,1,0:T(8,128)(2,1)S(1)} all-to-all(bf16[8,60,512]{2,1,0:T(8,128)(2,1)S(1)} %broadcast_select_fusion.1), channel_id=1, replica_groups=mesh['sp'=8,'tp'=4] {'sp'}, dimensions={0} | all-to-all | bytes 983040 | tf_op jit(solution)/shard_map/all_to_all | solution.py:101
  133.4 20.1 %all-gather.2.cloned.1.call-done = bf16[1,480,2048]{2,1,0:T(8,128)(2,1)} async-done(((bf16[1,480,512]{2,1,0:T(8,128)(2,1)}), bf16[1,480,2048]{2,1,0:T(8,128)(2,1)}) %all-gather.2.cloned.1.call-update) | async-done | bytes 1966096 | tf_op jit(solution)/shard_map/all_gather | solution.py:103
  153.6 2.7 %fusion.7 = f32[480,256]{1,0:T(8,128)S(1)} fusion(bf16[1,480,2048]{2,1,0:T(8,128)(2,1)} %all-gather.2.cloned.1.call-done, bf16[1,256,2048]{2,1,0:T(8,128)(2,1)} %param.26), kind=kOutput, calls=%fused_computation.12 | convolution fusion | flops 503316480 | bytes 3506176 | tf_op jit(solution)/shard_map/erd,efd->erf/dot_general | solution.py:104
  157.0 9.8 %all_gather.27 = bf16[480,1024]{1,0:T(8,128)(2,1)S(1)} all-gather(bf16[480,256]{1,0:T(8,128)(2,1)S(1)} %fusion.20), channel_id=1, replica_groups=mesh['sp'=8,'tp'=4] {'tp'}, dimensions={1}, use_global_device_ids=true | all-gather | bytes 1228800 | tf_op jit(solution)/shard_map/all_gather | solution.py:110
  168.9 3.7 %reduce.4 = bf16[480,512]{1,0:T(8,128)(2,1)S(1)} reduce(bf16[480,1,512]{2,1,0:T(2,128)(2,1)S(1)} %bitcast.81, bf16[]{:T(256)} %broadcast.119), dimensions={1}, to_apply=%bitcast.78.reduce_sub_computation | reduce | bytes 983042
  173.5 5.5 %all-to-all-start.1 = ((bf16[8,2,15360]{2,1,0:T(2,128)(2,1)}), bf16[8,2,15360]{2,1,0:T(2,128)(2,1)S(1)}, u32[]{:S(2)}, u32[]{:S(2)}) async-start(bf16[8,2,15360]{2,1,0:T(2,128)(2,1)} %reshape.198), calls=%async_computation.1 | async-start | bytes 983040 | tf_op jit(solution)/shard_map/all_to_all | solution.py:118
  179.3 1.7 fusion.43
  181.1 1.7 fusion.25
  182.8 6.3 %all_gather.25 = bf16[192,1024]{1,0:T(8,128)(2,1)S(1)} all-gather(bf16[192,256]{1,0:T(8,128)(2,1)S(1)} %fusion.25), channel_id=1, replica_groups=mesh['sp'=8,'tp'=4] {'tp'}, dimensions={1}, use_global_device_ids=true | all-gather | bytes 491520 | tf_op jit(solution)/shard_map/all_gather | solution.py:109
  189.1 4.2 %all-to-all-done.1 = bf16[8,2,15360]{2,1,0:T(2,128)(2,1)S(1)} async-done(((bf16[8,2,15360]{2,1,0:T(2,128)(2,1)}), bf16[8,2,15360]{2,1,0:T(2,128)(2,1)S(1)}, u32[]{:S(2)}, u32[]{:S(2)}) %all-to-all-start.1) | async-done | bytes 491552 | tf_op jit(solution)/shard_map/all_to_all | solution.py:118
  193.9 2.1 gather_fusion.1
  196.1 1.6 multiply_reduce_fusion
  197.7 2.0 fusion.24
  (75 shorter events, 11.3 us)
Async XLA Ops:
  6.5 160.3 %copy-start = (bf16[1,1024,512]{2,1,0:T(8,128)(2,1)S(1)}, bf16[1,1024,512]{2,1,0:T(8,128)(2,1)}, u32[]{:S(2)}) copy-start(bf16[1,1024,512]{2,1,0:T(8,128)(2,1)} %param.28) | copy-start | bytes 3145732
  6.5 147.0 %all-gather.2.cloned.1.call-start = ((), (), s32[]{:S(2)}) async-start(), calls=%async_computation.2 | async-start | bytes 2457600 | tf_op jit(solution)/shard_map/all_gather | solution.py:103
  50.5 4.5 %copy-start.2 = (bf16[192,256]{1,0:T(8,128)(2,1)S(1)}, bf16[192,256]{1,0:T(8,128)(2,1)}, u32[]{:S(2)}) copy-start(bf16[192,256]{1,0:T(8,128)(2,1)} %param.19) | copy-start | bytes 294916
  87.4 4.1 %copy-start.5 = (f32[4]{0:T(128)S(1)}, f32[4]{0:T(128)}, u32[]{:S(2)}) copy-start(f32[4]{0:T(128)} %param.20) | copy-start | bytes 52
  87.4 4.2 %copy-start.7 = (f32[64]{0:T(128)S(1)}, f32[64]{0:T(128)}, u32[]{:S(2)}) copy-start(f32[64]{0:T(128)} %param.21) | copy-start | bytes 772
  87.4 11.6 %copy-start.9 = (bf16[1024,512]{1,0:T(8,128)(2,1)S(1)}, bf16[1024,512]{1,0:T(8,128)(2,1)}, u32[]{:S(2)}) copy-start(bf16[1024,512]{1,0:T(8,128)(2,1)} %param.22) | copy-start | bytes 3145732
  87.4 11.5 %copy-start.11 = (bf16[192,512]{1,0:T(8,128)(2,1)S(1)}, bf16[192,512]{1,0:T(8,128)(2,1)}, u32[]{:S(2)}) copy-start(bf16[192,512]{1,0:T(8,128)(2,1)} %param.16) | copy-start | bytes 589828
  91.4 17.7 %copy-start.4 = (f32[2048]{0:T(1024)S(1)}, f32[2048]{0:T(1024)}, u32[]{:S(2)}) copy-start(f32[2048]{0:T(1024)} %param.23) | copy-start | bytes 24580
  133.3 22.9 %copy-start.10 = (bf16[1,256,2048]{2,1,0:T(8,128)(2,1)S(1)}, bf16[1,256,2048]{2,1,0:T(8,128)(2,1)}, u32[]{:S(2)}) copy-start(bf16[1,256,2048]{2,1,0:T(8,128)(2,1)} %param.27) | copy-start | bytes 3145732
  153.6 2.7 %copy-start.8 = (bf16[1,480,2048]{2,1,0:T(8,128)(2,1)S(1)}, bf16[1,480,2048]{2,1,0:T(8,128)(2,1)}, u32[]{:S(2)}) copy-start(bf16[1,480,2048]{2,1,0:T(8,128)(2,1)} %all-gather.2.cloned.1.call-done) | copy-start | bytes 5898244
  157.0 22.0 %copy-start.3 = (s32[192,2]{0,1:T(2,128)S(1)}, s32[192,2]{0,1:T(2,128)}, u32[]{:S(2)}) copy-start(s32[192,2]{0,1:T(2,128)} %param.24) | copy-start | bytes 4612
  157.0 22.2 %copy-start.6 = (f32[192,2]{0,1:T(2,128)S(1)}, f32[192,2]{0,1:T(2,128)}, u32[]{:S(2)}) copy-start(f32[192,2]{0,1:T(2,128)} %param.25) | copy-start | bytes 4612
  173.5 19.8 %all-to-all-start.1 = ((bf16[8,2,15360]{2,1,0:T(2,128)(2,1)}), bf16[8,2,15360]{2,1,0:T(2,128)(2,1)S(1)}, u32[]{:S(2)}, u32[]{:S(2)}) async-start(bf16[8,2,15360]{2,1,0:T(2,128)(2,1)} %reshape.198), calls=%async_computation.1 | async-start | bytes 983040 | tf_op jit(solution)/shard_map/all_to_all | solution.py:118
  193.9 3.9 %copy-start.1 = (bf16[1024,512]{1,0:T(8,128)(2,1)S(1)}, bf16[1024,512]{1,0:T(8,128)(2,1)}, u32[]{:S(2)}) copy-start(bf16[1024,512]{1,0:T(8,128)(2,1)} %param.31) | copy-start | bytes 3145732
Sparse Core Ops, SparseCore 0:
  133.3 20.2 all-gather.1
where the time goes:
time: 207 us
  blocking collectives  119 us (57%)
  waiting for transfers between devices  24.4 us (12%)
  matrix products  16.5 us (8%)
  local copies, waits for them, and re-layouts  15.1 us (7%)
  between operations  13.8 us (7%)
  other arithmetic  12.6 us (6%)
  starting transfers between devices  5.51 us (3%)
    all_gather x1, blocking collectives, body(): key_piece = lax.all_gather(key_rows, 'sp', axis=0, tiled=True)  34.1 us
    all_gather x1, blocking collectives, body(): value_piece = lax.all_gather(value_rows, 'sp', axis=0, tiled=True)  32.1 us
    all_to_all x1, blocking collectives, body(): lax.all_to_all(outgoing, 'sp', split_axis=0, concat_axis=1, tiled=True)  20.3 us
    all_gather x1, waiting for transfers between devices, body(): pieces = lax.all_gather(arrived, 'tp', axis=2, tiled=True)  20.1 us
    all_gather x1, blocking collectives, body(): lax.all_gather(expert_flat, 'tp', axis=1, tiled=True)  9.84 us
    all_gather x1, blocking collectives, body(): full_rows = lax.all_gather(hidden_state, 'tp', axis=1, tiled=True)  8.9 us
    all_gather x1, blocking collectives, body(): lax.all_gather(head_out, 'tp', axis=1, tiled=True)  7.21 us
    all_gather x1, blocking collectives, body(): lax.all_gather(shared_hidden, 'tp', axis=1, tiled=True)  6.29 us
  transfers between devices with their start and end apart: 2, of which 2 were waited for; matrix products, arithmetic and copies ran while one was open for 2% of the time, Pallas kernels for 0%

commit v1 on v0

--- a/solution.py
+++ b/solution.py
@@ -98,7 +98,10 @@
     own_cols = lax.dynamic_slice_in_dim(normed, lax.axis_index("tp") * col_dev, col_dev, 1)
     padded = jnp.concatenate([own_cols, jnp.zeros((1, col_dev), jnp.bfloat16)], axis=0)
     outgoing = jnp.take(padded, slot_token, axis=0).reshape(experts_all, capacity, col_dev)
-    arrived = lax.all_to_all(outgoing, "sp", split_axis=0, concat_axis=1, tiled=True)
+    arrived = jnp.concatenate(
+        lax.all_to_all(jnp.stack(jnp.split(outgoing, lax.axis_size("sp"), axis=0)), "sp", 0, 0),
+        axis=1,
+    )
     arrived_rows = arrived.shape[1]
     pieces = lax.all_gather(arrived, "tp", axis=2, tiled=True)
     gate_add = jnp.einsum("erd,efd->erf", pieces, expert_gate, preferred_element_type=jnp.float32)

time: 207 us -> 208 us (level)
    unnamed x31 -> x36, local copies, waits for them, and re-layouts: 4.14 us -> 4.22 us
where the time goes in v1:
time: 208 us
  blocking collectives  119 us (57%)
  waiting for transfers between devices  24.4 us (12%)
  matrix products  17.7 us (9%)
  local copies, waits for them, and re-layouts  15 us (7%)
  between operations  13.9 us (7%)
  other arithmetic  12.5 us (6%)
  starting transfers between devices  5.51 us (3%)
    all_gather x1, blocking collectives, body(): key_piece = lax.all_gather(key_rows, 'sp', axis=0, tiled=True)  34.1 us
    all_gather x1, blocking collectives, body(): value_piece = lax.all_gather(value_rows, 'sp', axis=0, tiled=True)  32.1 us
    all_to_all x1, blocking collectives, body(): lax.all_to_all(jnp.stack(jnp.split(outgoing, lax.axis_size('sp'), axis=0)...  20.3 us
    all_gather x1, waiting for transfers between devices, body(): pieces = lax.all_gather(arrived, 'tp', axis=2, tiled=True)  20.2 us
    all_gather x1, blocking collectives, body(): lax.all_gather(expert_flat, 'tp', axis=1, tiled=True)  9.84 us
    all_gather x1, blocking collectives, body(): full_rows = lax.all_gather(hidden_state, 'tp', axis=1, tiled=True)  8.9 us
    all_gather x1, blocking collectives, body(): lax.all_gather(head_out, 'tp', axis=1, tiled=True)  7.21 us
    all_gather x1, blocking collectives, body(): lax.all_gather(shared_hidden, 'tp', axis=1, tiled=True)  6.29 us
  transfers between devices with their start and end apart: 2, of which 2 were waited for; matrix products, arithmetic and copies ran while one was open for 2% of the time, Pallas kernels for 0%

profile of v1, /device:TPU:0, one launch (start us, length us, event | category | flops | bytes accessed | tf_op | source)
XLA Modules:
  0.0 207.8 jit_solution(3338166483786695574)
XLA Ops:
  10.1 2.9 %scatter_custom_fusion = s32[480]{0:T(512)S(1)} fusion(s32[384]{0:T(512)S(1)} %fusion.48, s32[384]{0:T(512)S(1)} %reshape.199, s32[]{:T(128)} %constant.26.clone.1), kind=kCustom, calls=%fused_computation.82 | custom fusion | bytes 1924 | tf_op jit(solution)/shard_map/scatter | solution.py:96
  13.3 34.1 %all_gather.21 = bf16[1536,256]{1,0:T(8,128)(2,1)S(1)} all-gather(bf16[192,256]{1,0:T(8,128)(2,1)} %param.18), channel_id=1, replica_groups=mesh['sp'=8,'tp'=4] {'sp'}, dimensions={0}, use_global_device_ids=true | all-gather | bytes 884736 | tf_op jit(solution)/shard_map/all_gather | solution.py:55
  48.6 1.9 fusion
  50.5 4.4 %fusion.1 = (f32[2,4,192]{2,1,0:T(4,128)S(1)}, bf16[2,4,192,1536]{3,2,1,0:T(8,128)(2,1)}) fusion(f32[2,4,192,1536]{3,2,1,0:T(8,128)S(1)} %get-tuple-element.8, f32[2,4,192]{2,1,0:T(4,128)S(1)} %broadcast_maximum_fusion, pred[192,1536]{1,0:T(8,128)(4,1)S(1)} %iota_compare_fusion), kind=kLoop, calls=%fused_computation.6 | loop fusion | flops 14154240 | bytes 14462976 | tf_op jit(solution)/shard_map/reduce_sum | solution.py:70
  55.0 32.1 %all_gather.22 = bf16[1536,256]{1,0:T(8,128)(2,1)S(1)} all-gather(bf16[192,256]{1,0:T(8,128)(2,1)S(1)} %copy-done.2), channel_id=1, replica_groups=mesh['sp'=8,'tp'=4] {'sp'}, dimensions={0}, use_global_device_ids=true | all-gather | bytes 884736 | tf_op jit(solution)/shard_map/all_gather | solution.py:56
  87.4 4.0 %fusion.29 = f32[2,4,192,64]{2,3,0,1:T(8,128)S(1)} fusion(bf16[1536,4,64,1]{0,2,3,1:T(8,128)(2,1)S(1)} %bitcast.116, bf16[2,4,192,1536]{3,2,1,0:T(8,128)(2,1)} %get-tuple-element.6, f32[2,4,192]{2,0,1:T(2,128)S(1)} %copy.66), kind=kOutput, calls=%fused_computation.35 | convolution fusion | flops 302088192 | bytes 5904384 | tf_op jit(solution)/shard_map/mhqk,khd->mhqd/dot_general | solution.py:71
  91.7 7.2 %all_gather.23 = bf16[192,1024]{0,1:T(8,128)(2,1)S(1)} all-gather(bf16[192,256]{0,1:T(8,128)(2,1)S(1)} %bitcast.117), channel_id=1, replica_groups=mesh['sp'=8,'tp'=4] {'tp'}, dimensions={1}, use_global_device_ids=true | all-gather | bytes 491520 | tf_op jit(solution)/shard_map/all_gather | solution.py:79
  98.9 1.1 fusion.23
  100.0 8.9 %all_gather.24 = bf16[192,2048]{1,0:T(8,128)(2,1)S(1)} all-gather(bf16[192,512]{1,0:T(8,128)(2,1)} %fusion.23), channel_id=1, replica_groups=mesh['sp'=8,'tp'=4] {'tp'}, dimensions={1}, use_global_device_ids=true | all-gather | bytes 983040 | tf_op jit(solution)/shard_map/all_gather | solution.py:84
  109.5 2.1 %gather_fusion = bf16[480,512]{1,0:T(8,128)(2,1)S(1)} fusion(bf16[193,512]{1,0:T(8,128)(2,1)S(1)} %concatenate.3, s32[1024]{0:T(1024)S(1)} %get-tuple-element.10), kind=kCustom, calls=%fused_computation | custom fusion | bytes 984960 | tf_op jit(solution)/shard_map/jit(_take)/gather | solution.py:100
  111.9 20.3 %all_to_all.14 = bf16[8,1,60,512]{3,2,1,0:T(8,128)(2,1)S(1)} all-to-all(bf16[8,1,60,512]{3,2,1,0:T(8,128)(2,1)S(1)} %fusion.37), channel_id=1, replica_groups=mesh['sp'=8,'tp'=4] {'sp'}, dimensions={0} | all-to-all | bytes 983040 | tf_op jit(solution)/shard_map/all_to_all | solution.py:102
  133.4 20.2 %all-gather.2.cloned.1.call-done = bf16[1,480,2048]{2,1,0:T(8,128)(2,1)} async-done(((bf16[1,480,512]{2,1,0:T(8,128)(2,1)}), bf16[1,480,2048]{2,1,0:T(8,128)(2,1)}) %all-gather.2.cloned.1.call-update) | async-done | bytes 1966096 | tf_op jit(solution)/shard_map/all_gather | solution.py:106
  153.5 2.7 %fusion.7 = f32[480,256]{1,0:T(8,128)S(1)} fusion(bf16[1,480,2048]{2,1,0:T(8,128)(2,1)} %all-gather.2.cloned.1.call-done, bf16[1,256,2048]{2,1,0:T(8,128)(2,1)} %param.26), kind=kOutput, calls=%fused_computation.12 | convolution fusion | flops 503316480 | bytes 3506176 | tf_op jit(solution)/shard_map/erd,efd->erf/dot_general | solution.py:107
  156.2 1.9 fusion.20
  158.2 9.8 %all_gather.27 = bf16[480,1024]{1,0:T(8,128)(2,1)S(1)} all-gather(bf16[480,256]{1,0:T(8,128)(2,1)S(1)} %fusion.20), channel_id=1, replica_groups=mesh['sp'=8,'tp'=4] {'tp'}, dimensions={1}, use_global_device_ids=true | all-gather | bytes 1228800 | tf_op jit(solution)/shard_map/all_gather | solution.py:113
  170.1 3.7 %reduce.4 = bf16[480,512]{1,0:T(8,128)(2,1)S(1)} reduce(bf16[480,1,512]{2,1,0:T(2,128)(2,1)S(1)} %bitcast.113, bf16[]{:T(256)} %broadcast.117), dimensions={1}, to_apply=%bitcast.110.reduce_sub_computation | reduce | bytes 983042
  174.7 5.5 %all-to-all-start.1 = ((bf16[8,2,15360]{2,1,0:T(2,128)(2,1)}), bf16[8,2,15360]{2,1,0:T(2,128)(2,1)S(1)}, u32[]{:S(2)}, u32[]{:S(2)}) async-start(bf16[8,2,15360]{2,1,0:T(2,128)(2,1)} %reshape.209), calls=%async_computation.1 | async-start | bytes 983040 | tf_op jit(solution)/shard_map/all_to_all | solution.py:121
  180.5 1.7 fusion.51
  182.3 1.7 fusion.25
  184.0 6.3 %all_gather.25 = bf16[192,1024]{1,0:T(8,128)(2,1)S(1)} all-gather(bf16[192,256]{1,0:T(8,128)(2,1)S(1)} %fusion.25), channel_id=1, replica_groups=mesh['sp'=8,'tp'=4] {'tp'}, dimensions={1}, use_global_device_ids=true | all-gather | bytes 491520 | tf_op jit(solution)/shard_map/all_gather | solution.py:112
  190.3 4.2 %all-to-all-done.1 = bf16[8,2,15360]{2,1,0:T(2,128)(2,1)S(1)} async-done(((bf16[8,2,15360]{2,1,0:T(2,128)(2,1)}), bf16[8,2,15360]{2,1,0:T(2,128)(2,1)S(1)}, u32[]{:S(2)}, u32[]{:S(2)}) %all-to-all-start.1) | async-done | bytes 491552 | tf_op jit(solution)/shard_map/all_to_all | solution.py:121
  195.1 2.1 gather_fusion.1
  197.3 1.6 multiply_reduce_fusion
  198.9 2.0 fusion.24
  (78 shorter events, 11.4 us)
Async XLA Ops:
  6.5 161.5 %copy-start = (bf16[1,1024,512]{2,1,0:T(8,128)(2,1)S(1)}, bf16[1,1024,512]{2,1,0:T(8,128)(2,1)}, u32[]{:S(2)}) copy-start(bf16[1,1024,512]{2,1,0:T(8,128)(2,1)} %param.28) | copy-start | bytes 3145732
  6.5 147.0 %all-gather.2.cloned.1.call-start = ((), (), s32[]{:S(2)}) async-start(), calls=%async_computation.2 | async-start | bytes 2457600 | tf_op jit(solution)/shard_map/all_gather | solution.py:106
  50.5 4.5 %copy-start.2 = (bf16[192,256]{1,0:T(8,128)(2,1)S(1)}, bf16[192,256]{1,0:T(8,128)(2,1)}, u32[]{:S(2)}) copy-start(bf16[192,256]{1,0:T(8,128)(2,1)} %param.19) | copy-start | bytes 294916
  87.4 4.1 %copy-start.5 = (f32[4]{0:T(128)S(1)}, f32[4]{0:T(128)}, u32[]{:S(2)}) copy-start(f32[4]{0:T(128)} %param.20) | copy-start | bytes 52
  87.4 4.2 %copy-start.7 = (f32[64]{0:T(128)S(1)}, f32[64]{0:T(128)}, u32[]{:S(2)}) copy-start(f32[64]{0:T(128)} %param.21) | copy-start | bytes 772
  87.4 11.6 %copy-start.9 = (bf16[1024,512]{1,0:T(8,128)(2,1)S(1)}, bf16[1024,512]{1,0:T(8,128)(2,1)}, u32[]{:S(2)}) copy-start(bf16[1024,512]{1,0:T(8,128)(2,1)} %param.22) | copy-start | bytes 3145732
  87.4 11.5 %copy-start.10 = (bf16[192,512]{1,0:T(8,128)(2,1)S(1)}, bf16[192,512]{1,0:T(8,128)(2,1)}, u32[]{:S(2)}) copy-start(bf16[192,512]{1,0:T(8,128)(2,1)} %param.16) | copy-start | bytes 589828
  91.4 17.7 %copy-start.4 = (f32[2048]{0:T(1024)S(1)}, f32[2048]{0:T(1024)}, u32[]{:S(2)}) copy-start(f32[2048]{0:T(1024)} %param.23) | copy-start | bytes 24580
  153.5 2.7 %copy-start.8 = (bf16[1,480,2048]{2,1,0:T(8,128)(2,1)S(1)}, bf16[1,480,2048]{2,1,0:T(8,128)(2,1)}, u32[]{:S(2)}) copy-start(bf16[1,480,2048]{2,1,0:T(8,128)(2,1)} %all-gather.2.cloned.1.call-done) | copy-start | bytes 5898244
  158.2 22.1 %copy-start.3 = (s32[192,2]{0,1:T(2,128)S(1)}, s32[192,2]{0,1:T(2,128)}, u32[]{:S(2)}) copy-start(s32[192,2]{0,1:T(2,128)} %param.24) | copy-start | bytes 4612
  158.2 22.2 %copy-start.6 = (f32[192,2]{0,1:T(2,128)S(1)}, f32[192,2]{0,1:T(2,128)}, u32[]{:S(2)}) copy-start(f32[192,2]{0,1:T(2,128)} %param.25) | copy-start | bytes 4612
  174.7 19.8 %all-to-all-start.1 = ((bf16[8,2,15360]{2,1,0:T(2,128)(2,1)}), bf16[8,2,15360]{2,1,0:T(2,128)(2,1)S(1)}, u32[]{:S(2)}, u32[]{:S(2)}) async-start(bf16[8,2,15360]{2,1,0:T(2,128)(2,1)} %reshape.209), calls=%async_computation.1 | async-start | bytes 983040 | tf_op jit(solution)/shard_map/all_to_all | solution.py:121
  195.1 3.9 %copy-start.1 = (bf16[1024,512]{1,0:T(8,128)(2,1)S(1)}, bf16[1024,512]{1,0:T(8,128)(2,1)}, u32[]{:S(2)}) copy-start(bf16[1024,512]{1,0:T(8,128)(2,1)} %param.31) | copy-start | bytes 3145732
Sparse Core Ops, SparseCore 0:
  133.3 20.2 all-gather.1
